TPU v7x, 32 devices: a whole 2x2x4 slice. The times are simulated.
32 devices in a mesh: sp: 8 (over z, x), dp: 4 (over y, core).
Axes of the slice: x: 2, y: 2, z: 4, core: 2. Of those that a mesh axis runs over, the one named last changes fastest.
Arguments:
- layer_activity: bfloat16 [4, 1024, 2048], P('dp', 'sp'), may hold values from -6 to 6
- writer_matrix: bfloat16 [2048, 256], P('dp'), may hold values from -0.125 to 0.125
- reader_matrix: bfloat16 [2048, 256], P('dp'), may hold values from -0.125 to 0.125
- source_unfiltered: bfloat16 [4, 1024, 2048], P('dp', 'sp'), may hold values from -6 to 6
- switch_raw_signal: bfloat16 [4, 1024, 2048], P('dp', 'sp'), may hold values from -6 to 6
- saved_result: bfloat16 [4, 1024, 2048], P('dp', 'sp'), may hold values from -6 to 6
- final_adjoint: bfloat16 [4, 1024, 2048], P('dp', 'sp'), may hold values from -6 to 6
- delta_raw: bfloat16 [4, 1024, 32], P('dp', 'sp'), may hold values from -4 to 4
- extra_logdrop: float32 [4, 1024, 32], P('dp', None, 'sp'), may hold values from 0 to 2.1
- source_filter_coefs: float32 [5, 2048], P(None, 'sp'), may hold values from -2.5 to 2.5
- writer_filter_coefs: float32 [5, 256], replicated, may hold values from -2.5 to 2.5
- reader_filter_coefs: float32 [5, 256], replicated, may hold values from -2.5 to 2.5
- delta_offset: float32 [32], P('sp'), may hold values from -7.5 to -6
- fading_exponents: float32 [32], P('sp'), may hold values from -6 to 3.4
- direct_factor: float32 [32], P('sp'), may hold values from 0.1 to 1.9
- rescale_factor: float32 [2048], replicated, may hold values from 0.1 to 1.9
Outputs:
- d_hidden: bfloat16 [4, 1024, 2048], P('dp', 'sp')
- d_x_raw: bfloat16 [4, 1024, 2048], P('dp', 'sp')
- d_gate: bfloat16 [4, 1024, 2048], P('dp', 'sp')
- d_dt_raw: bfloat16 [4, 1024, 32], P('dp', 'sp')
- d_w_b: float32 [2048, 256], P('dp')
- d_w_c: float32 [2048, 256], P('dp')
All inputs are finite; a program needn't handle non-finite values.
Results may differ from a plain program's by a relative error of at most 0.012.
Values may be sent and summed in bfloat16 or wider, within the bound.
A program may use at most 128 MiB of HBM per device.

v0:
```python
import jax
import jax.numpy as jnp
from jax import lax
from jax.sharding import PartitionSpec as P

HEADS = 32
HEAD_DIM = 64
STATE = 128
GROUPS = 2
NORM_GROUPS = 8
CONV_K = 5
BLOCK = 128
INNER = 2048
EPSILON = 1e-06
highest = lax.Precision.HIGHEST


def centred_conv(values, tap_weights):
    sample_window = values.shape[0]
    reach_side = (tap_weights.shape[0] - 1) // 2
    padded = jnp.pad(values, ((reach_side, reach_side), (0, 0)))
    summed = jnp.zeros_like(values)
    for offset in range(tap_weights.shape[0]):
        summed = summed + tap_weights[offset][None, :] * padded[offset : offset + sample_window]
    return summed


def one_channel_scan(
    source_unfiltered,
    writer_unfiltered,
    reader_unfiltered,
    delta_raw,
    extra_logdrop,
    source_filter_coefs,
    writer_filter_coefs,
    reader_filter_coefs,
    delta_offset,
    fading_exponents,
    direct_factor,
):
    inputs = jax.nn.silu(centred_conv(source_unfiltered, source_filter_coefs))
    keys_b = jax.nn.silu(centred_conv(writer_unfiltered, writer_filter_coefs))
    reads_c = jax.nn.silu(centred_conv(reader_unfiltered, reader_filter_coefs))
    smooth_delta = jax.nn.softplus(delta_raw + delta_offset)
    channel_fading = smooth_delta * jnp.exp(fading_exponents) + extra_logdrop
    cumulative = jnp.cumsum(channel_fading)
    sample_window = source_unfiltered.shape[0]
    blocks = sample_window // BLOCK
    driven = (inputs * smooth_delta[:, None]).reshape(blocks, BLOCK, -1)
    keyed = keys_b.reshape(blocks, BLOCK, -1)
    reading = reads_c.reshape(blocks, BLOCK, -1)
    levels = cumulative.reshape(blocks, BLOCK)
    within = jnp.exp(-jnp.abs(levels[:, :, None] - levels[:, None, :]))
    scores = jnp.einsum("ktn,ksn->kts", reading, keyed, precision=highest) * within
    output = jnp.einsum("kts,ksp->ktp", scores, driven, precision=highest)
    block_ends = levels[:, -1]
    block_starts = levels[:, 0]
    block_order = jnp.arange(blocks, dtype=jnp.int32)
    prev_end = jnp.concatenate([cumulative[:1], block_ends[:-1]])
    next_start = jnp.concatenate([block_starts[1:], cumulative[-1:]])
    weight_fwd = jnp.exp(levels - block_ends[:, None])
    state_fwd = jnp.einsum(
        "ksn,ksp->knp", keyed * weight_fwd[:, :, None], driven, precision=highest
    )
    mask_fwd = (block_order[None, :] < block_order[:, None]).astype(cumulative.dtype)
    link_fwd = jnp.exp(-jnp.abs(prev_end[:, None] - block_ends[None, :])) * mask_fwd
    carry_fwd = jnp.einsum("kj,jnp->knp", link_fwd, state_fwd, precision=highest)
    read_fwd = reading * jnp.exp(prev_end[:, None] - levels)[:, :, None]
    weight_bwd = jnp.exp(block_starts[:, None] - levels)
    state_bwd = jnp.einsum(
        "ksn,ksp->knp", keyed * weight_bwd[:, :, None], driven, precision=highest
    )
    mask_bwd = (block_order[None, :] > block_order[:, None]).astype(cumulative.dtype)
    link_bwd = jnp.exp(-jnp.abs(next_start[:, None] - block_starts[None, :])) * mask_bwd
    carry_bwd = jnp.einsum("kj,jnp->knp", link_bwd, state_bwd, precision=highest)
    read_bwd = reading * jnp.exp(levels - next_start[:, None])[:, :, None]
    output = output + jnp.einsum("ktn,knp->ktp", read_fwd, carry_fwd, precision=highest)
    output = output + jnp.einsum("ktn,knp->ktp", read_bwd, carry_bwd, precision=highest)
    return output.reshape(sample_window, -1) + direct_factor * inputs


def channelwise_derivs(
    source_unfiltered,
    writer_unfiltered,
    reader_unfiltered,
    delta_raw,
    extra_logdrop,
    source_filter_coefs,
    writer_filter_coefs,
    reader_filter_coefs,
    delta_offset,
    fading_exponents,
    direct_factor,
    result_adjoint,
):

    def forward(source_filtered, writer_filtered, reader_filtered, delta_argument):
        return one_channel_scan(
            source_filtered,
            writer_filtered,
            reader_filtered,
            delta_argument,
            extra_logdrop,
            source_filter_coefs,
            writer_filter_coefs,
            reader_filter_coefs,
            delta_offset,
            fading_exponents,
            direct_factor,
        )

    primal, pullback = jax.vjp(
        forward,
        source_unfiltered.astype(jnp.float32),
        writer_unfiltered.astype(jnp.float32),
        reader_unfiltered.astype(jnp.float32),
        delta_raw.astype(jnp.float32),
    )
    source_derivative, writer_derivative, reader_derivative, delta_derivative = pullback(
        result_adjoint.astype(jnp.float32)
    )
    return (
        source_derivative.astype(jnp.bfloat16),
        writer_derivative.astype(jnp.bfloat16),
        reader_derivative.astype(jnp.bfloat16),
        delta_derivative.astype(jnp.bfloat16),
    )


def gated_norm(values, gating, rescale_factor):
    mixed = values * jax.nn.silu(gating)
    grouped = mixed.reshape(mixed.shape[0], NORM_GROUPS, -1)
    scaled = grouped * lax.rsqrt(jnp.mean(grouped * grouped, axis=-1, keepdims=True) + EPSILON)
    return scaled.reshape(mixed.shape) * rescale_factor


def norm_backward(saved_result, switch_raw_signal, final_adjoint, rescale_factor):
    primal, pullback = jax.vjp(
        lambda values, gating: gated_norm(values, gating, rescale_factor),
        saved_result.astype(jnp.float32),
        switch_raw_signal.astype(jnp.float32),
    )
    d_values, d_gates = pullback(final_adjoint.astype(jnp.float32))
    return (d_values.astype(jnp.bfloat16), d_gates.astype(jnp.bfloat16))


def spread_heads(columns, tokens):
    grouped = columns.reshape(tokens, GROUPS, 1, STATE)
    copied = jnp.broadcast_to(grouped, (tokens, GROUPS, HEADS // GROUPS, STATE))
    return copied.reshape(1, tokens, HEADS * STATE)


def heads_first(values, window, local_channels, width):
    return jnp.transpose(values.reshape(window, local_channels, width), (1, 0, 2))


def local(
    layer_activity,
    writer_matrix,
    reader_matrix,
    source_unfiltered,
    switch_raw_signal,
    saved_result,
    final_adjoint,
    delta_raw,
    extra_logdrop,
    source_filter_coefs,
    writer_filter_coefs,
    reader_filter_coefs,
    delta_offset,
    fading_exponents,
    direct_factor,
    rescale_factor,
):
    tokens = layer_activity.shape[1]
    width_in = layer_activity.shape[2]
    latent_dimension = GROUPS * STATE
    data_devices = lax.axis_size("dp")
    local_channels = delta_offset.shape[0]
    per_group = HEADS // GROUPS
    weights = lax.all_gather(
        jnp.concatenate([writer_matrix, reader_matrix], axis=1), "dp", axis=0, tiled=True
    )
    token_rows = layer_activity.reshape(tokens, width_in)
    projected = jnp.dot(token_rows, weights, preferred_element_type=jnp.float32).astype(
        jnp.bfloat16
    )
    result_adjoint, d_gate = norm_backward(
        saved_result.reshape(tokens, INNER),
        switch_raw_signal.reshape(tokens, INNER),
        final_adjoint.reshape(tokens, INNER),
        rescale_factor,
    )
    copies_b = spread_heads(projected[:, :latent_dimension], tokens)
    copies_c = spread_heads(projected[:, latent_dimension:], tokens)
    heads_x, heads_b, heads_c, heads_dt, heads_dy = (
        lax.all_to_all(source_unfiltered, "sp", split_axis=2, concat_axis=1, tiled=True),
        lax.all_to_all(copies_b, "sp", split_axis=2, concat_axis=1, tiled=True),
        lax.all_to_all(copies_c, "sp", split_axis=2, concat_axis=1, tiled=True),
        lax.all_to_all(delta_raw, "sp", split_axis=2, concat_axis=1, tiled=True),
        lax.all_to_all(
            result_adjoint.reshape(1, tokens, INNER), "sp", split_axis=2, concat_axis=1, tiled=True
        ),
    )
    window = heads_x.shape[1]
    first_head = lax.axis_index("sp") * local_channels
    head_ids = first_head + jnp.arange(local_channels, dtype=jnp.int32)
    chooser = (
        head_ids[:, None] // per_group == jnp.arange(GROUPS, dtype=jnp.int32)[None, :]
    ).astype(jnp.float32)
    writer_filter_fn = jnp.einsum(
        "kgn,hg->hkn",
        writer_filter_coefs.reshape(CONV_K, GROUPS, STATE),
        chooser,
        precision=highest,
    )
    reader_filter_fn = jnp.einsum(
        "kgn,hg->hkn",
        reader_filter_coefs.reshape(CONV_K, GROUPS, STATE),
        chooser,
        precision=highest,
    )
    source_filter_fn = jnp.transpose(
        source_filter_coefs.reshape(CONV_K, local_channels, HEAD_DIM), (1, 0, 2)
    )
    per_head = jax.vmap(channelwise_derivs)
    source_derivative, writer_derivative, reader_derivative, delta_derivative = per_head(
        heads_first(heads_x, window, local_channels, HEAD_DIM),
        heads_first(heads_b, window, local_channels, STATE),
        heads_first(heads_c, window, local_channels, STATE),
        heads_dt.reshape(window, local_channels).T,
        extra_logdrop.reshape(window, local_channels).T,
        source_filter_fn,
        writer_filter_fn,
        reader_filter_fn,
        delta_offset,
        fading_exponents,
        direct_factor,
        heads_first(heads_dy, window, local_channels, HEAD_DIM),
    )
    back_x, back_b, back_c, back_dt = (
        lax.all_to_all(
            jnp.transpose(source_derivative, (1, 0, 2)).reshape(
                1, window, local_channels * HEAD_DIM
            ),
            "sp",
            split_axis=1,
            concat_axis=2,
            tiled=True,
        ),
        lax.all_to_all(
            jnp.transpose(writer_derivative, (1, 0, 2)).reshape(1, window, local_channels * STATE),
            "sp",
            split_axis=1,
            concat_axis=2,
            tiled=True,
        ),
        lax.all_to_all(
            jnp.transpose(reader_derivative, (1, 0, 2)).reshape(1, window, local_channels * STATE),
            "sp",
            split_axis=1,
            concat_axis=2,
            tiled=True,
        ),
        lax.all_to_all(
            delta_derivative.T.reshape(1, window, local_channels),
            "sp",
            split_axis=1,
            concat_axis=2,
            tiled=True,
        ),
    )
    summed_b = jnp.sum(back_b.reshape(tokens, GROUPS, per_group, STATE).astype(jnp.float32), axis=2)
    summed_c = jnp.sum(back_c.reshape(tokens, GROUPS, per_group, STATE).astype(jnp.float32), axis=2)
    gradients = jnp.concatenate(
        [
            summed_b.reshape(tokens, latent_dimension).astype(jnp.bfloat16),
            summed_c.reshape(tokens, latent_dimension).astype(jnp.bfloat16),
        ],
        axis=1,
    )
    d_hidden = jnp.einsum(
        "tc,dc->td", gradients, weights, preferred_element_type=jnp.float32
    ).astype(jnp.bfloat16)
    column_block = lax.all_to_all(layer_activity, "dp", split_axis=2, concat_axis=0, tiled=True)
    all_columns = column_block.reshape(data_devices * tokens, width_in // data_devices)
    all_grads = lax.all_gather(gradients, "dp", axis=0, tiled=True)
    local_rows = jnp.einsum("td,tc->dc", all_columns, all_grads, preferred_element_type=jnp.float32)
    total_grad = lax.psum(local_rows, "sp")
    return (
        d_hidden.reshape(1, tokens, width_in),
        back_x,
        d_gate.reshape(1, tokens, INNER),
        back_dt,
        total_grad[:, :latent_dimension],
        total_grad[:, latent_dimension:],
    )


def solution(mesh):
    in_specs = (
        P("dp", "sp", None),
        P("dp", None),
        P("dp", None),
        P("dp", "sp", None),
        P("dp", "sp", None),
        P("dp", "sp", None),
        P("dp", "sp", None),
        P("dp", "sp", None),
        P("dp", None, "sp"),
        P(None, "sp"),
        P(),
        P(),
        P("sp"),
        P("sp"),
        P("sp"),
        P(),
    )
    out_specs = (
        P("dp", "sp", None),
        P("dp", "sp", None),
        P("dp", "sp", None),
        P("dp", "sp", None),
        P("dp", None),
        P("dp", None),
    )
    return jax.shard_map(local, mesh=mesh, in_specs=in_specs, out_specs=out_specs, check_vma=False)
```

profile of v0, /device:TPU:0, one launch (start us, length us, event | category | flops | bytes accessed | tf_op | source)
XLA Modules:
  0.0 509.0 jit_solution(16484277088458486737)
XLA Ops:
  11.6 7.3 %all-to-all-start.1 = ((bf16[8,2,256]{2,1,0:T(2,128)(2,1)}), bf16[8,2,256]{2,1,0:T(2,128)(2,1)S(1)}, u32[]{:S(2)}, u32[]{:S(2)}) async-start(bf16[8,2,256]{2,1,0:T(2,128)(2,1)} %reshape.408), calls=%async_computation.1 | async-start | bytes 16384 | tf_op jit(solution)/shard_map/all_to_all | solution.py:200
  21.4 11.6 %reduce.19 = bf16[2048,128]{1,0:T(8,128)(2,1)S(1)} reduce(bf16[2048,1,128]{2,1,0:T(2,128)(2,1)S(1)} %bitcast.410, bf16[]{:T(256)} %broadcast.265), dimensions={1}, to_apply=%bitcast.316.reduce_sub_computation | reduce | bytes 1048578
  38.1 11.6 %reduce.14 = bf16[2048,128]{1,0:T(8,128)(2,1)S(1)} reduce(bf16[2048,1,128]{2,1,0:T(2,128)(2,1)S(1)} %bitcast.411, bf16[]{:T(256)} %broadcast.265), dimensions={1}, to_apply=%bitcast.304.reduce_sub_computation | reduce | bytes 1048578
  51.3 6.3 %all-to-all-start = ((bf16[8,2,16384]{2,1,0:T(2,128)(2,1)}), bf16[8,2,16384]{2,1,0:T(2,128)(2,1)}, u32[]{:S(2)}, u32[]{:S(2)}) async-start(bf16[8,2,16384]{2,1,0:T(2,128)(2,1)} %reshape.410), calls=%async_computation | async-start | bytes 1048576 | tf_op jit(solution)/shard_map/all_to_all | solution.py:197
  64.4 11.6 %reduce.13 = bf16[2048,128]{1,0:T(8,128)(2,1)S(1)} reduce(bf16[2048,1,128]{2,1,0:T(2,128)(2,1)S(1)} %bitcast.407, bf16[]{:T(256)} %broadcast.265), dimensions={1}, to_apply=%bitcast.306.reduce_sub_computation | reduce | bytes 1048578
  76.9 6.3 %all-to-all-start.3 = ((bf16[8,2,16384]{2,1,0:T(2,128)(2,1)}), bf16[8,2,16384]{2,1,0:T(2,128)(2,1)}, u32[]{:S(2)}, u32[]{:S(2)}) async-start(bf16[8,2,16384]{2,1,0:T(2,128)(2,1)} %reshape.412), calls=%async_computation.3 | async-start | bytes 1048576 | tf_op jit(solution)/shard_map/all_to_all | solution.py:201
  86.1 16.7 %copy.538 = bf16[1,128,4096]{1,0,2:T(2,128)(2,1)S(1)} copy(bf16[1,128,4096]{1,2,0:T(8,128)(2,1)S(1)} %bitcast.397) | data formatting | bytes 2097152 | tf_op jit(solution)/shard_map/reshape | solution.py:150
  102.8 22.4 %reduce.11 = bf16[4096,128]{1,0:T(8,128)(2,1)S(1)} reduce(bf16[4096,1,128]{2,1,0:T(2,128)(2,1)S(1)} %bitcast.391, bf16[]{:T(256)} %broadcast.265), dimensions={1}, to_apply=%bitcast.364.reduce_sub_computation | reduce | bytes 2097154
  126.4 6.5 %all-to-all-start.4 = ((bf16[8,2,32768]{2,1,0:T(2,128)(2,1)}), bf16[8,2,32768]{2,1,0:T(2,128)(2,1)S(1)}, u32[]{:S(2)}, u32[]{:S(2)}) async-start(bf16[8,2,32768]{2,1,0:T(2,128)(2,1)} %reshape.406), calls=%async_computation.4 | async-start | bytes 2097152 | tf_op jit(solution)/shard_map/all_to_all | solution.py:198
  135.3 16.7 %copy.539 = bf16[1,128,4096]{1,0,2:T(2,128)(2,1)S(1)} copy(bf16[1,128,4096]{1,2,0:T(8,128)(2,1)S(1)} %bitcast.398) | data formatting | bytes 2097152 | tf_op jit(solution)/shard_map/reshape | solution.py:150
  152.1 23.3 %reduce.10 = bf16[4096,128]{1,0:T(8,128)(2,1)} reduce(bf16[4096,1,128]{2,1,0:T(2,128)(2,1)S(1)} %bitcast.392, bf16[]{:T(256)} %broadcast.265), dimensions={1}, to_apply=%bitcast.365.reduce_sub_computation | reduce | bytes 2097154
  177.7 6.2 %all-to-all-start.2 = ((bf16[8,2,32768]{2,1,0:T(2,128)(2,1)}), bf16[8,2,32768]{2,1,0:T(2,128)(2,1)}, u32[]{:S(2)}, u32[]{:S(2)}) async-start(bf16[8,2,32768]{2,1,0:T(2,128)(2,1)} %reshape.404), calls=%async_computation.2 | async-start | bytes 2097152 | tf_op jit(solution)/shard_map/all_to_all | solution.py:199
  265.1 6.4 %fusion.208 = (f32[4,8,128]{2,1,0:T(8,128)S(1)}, f32[4,8,128]{2,1,0:T(8,128)S(1)}, f32[4,8,128,128]{3,2,1,0:T(8,128)}) fusion(f32[4,8,128,128]{3,2,1,0:T(8,128)S(1)} %copy-done.5, f32[4,8,128,128]{3,2,1,0:T(8,128)S(1)} %bitcast.380, f32[4,8,128,128]{3,2,1,0:T(8,128)S(1)} %bitcast.374, f32[4,8,128]{2,1,0:T(8,128)S(1)} %broadcast_add_fusion), kind=kOutput, calls=%fused_computation.322 | convolution fusion | flops 812113920 | bytes 8437760 | tf_op jit(solution)/shard_map/vmap(jvp(ktn,ksn->kts))/dot_general | solution.py:54
  271.4 6.6 %add_add_fusion.1 = f32[4,8,128,128]{3,2,1,0:T(8,128)} fusion(f32[4,8,128,128]{3,2,1,0:T(8,128)S(1)} %copy-done.6, f32[4,8,128,128]{3,2,1,0:T(8,128)S(1)} %get-tuple-element.122, f32[4,8,128,128]{3,2,1,0:T(8,128)S(1)} %bitcast.381, f32[4,8,128,128]{3,2,1,0:T(8,128)S(1)} %copy-done.5, f32[4,8,128]{2,1,0:T(8,128)S(1)} %broadcast_add_fusion, ...), kind=kOutput, calls=%fused_computation.64 | convolution fusion | flops 809500672 | bytes 10534912 | tf_op jit(solution)/shard_map/vmap(transpose(jvp(ktn,ksn->kts)))/dot_general | solution.py:54
  295.9 6.0 %copy.372 = bf16[1,1024,512]{2,0,1:T(2,128)(2,1)} copy(bf16[1,1024,512]{1,2,0:T(8,128)(2,1)} %bitcast.413) | data formatting | bytes 2097152 | tf_op jit(solution)/shard_map/reshape | solution.py:259
  301.9 9.0 %reduce.15 = bf16[1024,512]{1,0:T(8,128)(2,1)} reduce(bf16[1024,1,512]{2,1,0:T(2,128)(2,1)} %bitcast.393, bf16[]{:T(256)} %broadcast.265), dimensions={1}, to_apply=%bitcast.308.reduce_sub_computation | reduce | bytes 2097154
  333.3 5.9 %copy.359 = bf16[1,1024,512]{2,0,1:T(2,128)(2,1)} copy(bf16[1,1024,512]{1,2,0:T(8,128)(2,1)} %bitcast.414) | data formatting | bytes 2097152 | tf_op jit(solution)/shard_map/reshape | solution.py:252
  339.3 9.0 %reduce.16 = bf16[1024,512]{1,0:T(8,128)(2,1)} reduce(bf16[1024,1,512]{2,1,0:T(2,128)(2,1)} %bitcast.394, bf16[]{:T(256)} %broadcast.265), dimensions={1}, to_apply=%bitcast.310.reduce_sub_computation | reduce | bytes 2097154
  355.2 6.0 %all-to-all-start.5 = ((bf16[8,2,32768]{2,1,0:T(2,128)(2,1)}), bf16[8,2,32768]{2,1,0:T(2,128)(2,1)}, u32[]{:S(2)}, u32[]{:S(2)}) async-start(bf16[8,2,32768]{2,1,0:T(2,128)(2,1)} %reshape.416), calls=%async_computation.5 | async-start | bytes 2097152 | tf_op jit(solution)/shard_map/all_to_all | solution.py:251
  388.8 6.0 %all-to-all-start.8 = ((bf16[8,2,256]{2,1,0:T(2,128)(2,1)}), bf16[8,2,256]{2,1,0:T(2,128)(2,1)S(1)}, u32[]{:S(2)}, u32[]{:S(2)}) async-start(bf16[8,2,256]{2,1,0:T(2,128)(2,1)} %reshape.420), calls=%async_computation.8 | async-start | bytes 16384 | tf_op jit(solution)/shard_map/all_to_all | solution.py:265
  400.9 7.3 %all_gather.7 = bf16[512,512]{0,1:T(8,128)(2,1)S(1)} all-gather(bf16[128,512]{0,1:T(8,128)(2,1)S(1)} %pad_maximum_fusion.1), channel_id=1, replica_groups=mesh['sp'=8,'dp'=4] {'dp'}, dimensions={0}, use_global_device_ids=true | all-gather | bytes 655360 | tf_op jit(solution)/shard_map/all_gather | solution.py:287
  408.3 6.0 %all-to-all-start.7 = ((bf16[8,2,16384]{2,1,0:T(2,128)(2,1)}), bf16[8,2,16384]{2,1,0:T(2,128)(2,1)S(1)}, u32[]{:S(2)}, u32[]{:S(2)}) async-start(bf16[8,2,16384]{2,1,0:T(2,128)(2,1)} %reshape.418), calls=%async_computation.7 | async-start | bytes 1048576 | tf_op jit(solution)/shard_map/all_to_all | solution.py:242
  417.4 17.0 %all-to-all-done.7 = bf16[8,2,16384]{2,1,0:T(2,128)(2,1)S(1)} async-done(((bf16[8,2,16384]{2,1,0:T(2,128)(2,1)}), bf16[8,2,16384]{2,1,0:T(2,128)(2,1)S(1)}, u32[]{:S(2)}, u32[]{:S(2)}) %all-to-all-start.7) | async-done | bytes 524320 | tf_op jit(solution)/shard_map/all_to_all | solution.py:242
  439.7 58.7 %all-reduce.26.cloned.1.call-done = f32[512,512]{0,1:T(8,128)} async-done(((f32[512,512]{0,1:T(8,128)}), f32[512,512]{0,1:T(8,128)}) %all-reduce.26.cloned.1.call-update) | async-done | bytes 1048592 | tf_op jit(solution)/shard_map/psum | solution.py:289
  (250 shorter events, 203.0 us)
Async XLA Ops:
  7.2 76.3 %all-gather.2.cloned.1.call-start = ((), (), s32[]{:S(2)}) async-start(), calls=%async_computation.10 | async-start | bytes 2621440 | tf_op jit(solution)/shard_map/all_gather | solution.py:181
  11.6 22.2 %all-to-all-start.1 = ((bf16[8,2,256]{2,1,0:T(2,128)(2,1)}), bf16[8,2,256]{2,1,0:T(2,128)(2,1)S(1)}, u32[]{:S(2)}, u32[]{:S(2)}) async-start(bf16[8,2,256]{2,1,0:T(2,128)(2,1)} %reshape.408), calls=%async_computation.1 | async-start | bytes 16384 | tf_op jit(solution)/shard_map/all_to_all | solution.py:200
  21.3 16.0 %copy-start.28 = (f32[2048]{0:T(1024)S(1)}, f32[2048]{0:T(1024)}, u32[]{:S(2)}) copy-start(f32[2048]{0:T(1024)} %param.31) | copy-start | bytes 24580
  21.3 16.0 %copy-start.27 = (bf16[1,128,2048]{2,1,0:T(8,128)(2,1)S(1)}, bf16[1,128,2048]{2,1,0:T(8,128)(2,1)}, u32[]{:S(2)}) copy-start(bf16[1,128,2048]{2,1,0:T(8,128)(2,1)} %param.19) | copy-start | bytes 1572868
  33.8 17.5 %all-to-all-start.9 = ((bf16[4,2,32768]{2,1,0:T(2,128)(2,1)}), bf16[4,2,32768]{2,1,0:T(2,128)(2,1)S(1)}, u32[]{:S(2)}, u32[]{:S(2)}) async-start(bf16[4,2,32768]{2,1,0:T(2,128)(2,1)} %reshape.422), calls=%async_computation.9 | async-start | bytes 1048576 | tf_op jit(solution)/shard_map/all_to_all | solution.py:285
  37.3 13.3 %copy-start.22 = (bf16[1,128,2048]{2,1,0:T(8,128)(2,1)S(1)}, bf16[1,128,2048]{2,1,0:T(8,128)(2,1)}, u32[]{:S(2)}) copy-start(bf16[1,128,2048]{2,1,0:T(8,128)(2,1)} %param.22) | copy-start | bytes 1572868
  38.1 12.6 %copy-start.21 = (bf16[1,128,2048]{2,1,0:T(8,128)(2,1)S(1)}, bf16[1,128,2048]{2,1,0:T(8,128)(2,1)}, u32[]{:S(2)}) copy-start(bf16[1,128,2048]{2,1,0:T(8,128)(2,1)} %param.21) | copy-start | bytes 1572868
  51.3 25.6 %all-to-all-start = ((bf16[8,2,16384]{2,1,0:T(2,128)(2,1)}), bf16[8,2,16384]{2,1,0:T(2,128)(2,1)}, u32[]{:S(2)}, u32[]{:S(2)}) async-start(bf16[8,2,16384]{2,1,0:T(2,128)(2,1)} %reshape.410), calls=%async_computation | async-start | bytes 1048576 | tf_op jit(solution)/shard_map/all_to_all | solution.py:197
  64.4 19.1 %copy-start.25 = (bf16[1,128,2048]{2,1,0:T(8,128)(2,1)S(1)}, bf16[1,128,2048]{2,1,0:T(8,128)(2,1)}, u32[]{:S(2)}) copy-start(bf16[1,128,2048]{2,1,0:T(8,128)(2,1)} %param.16) | copy-start | bytes 1572868
  76.9 49.5 %all-to-all-start.3 = ((bf16[8,2,16384]{2,1,0:T(2,128)(2,1)}), bf16[8,2,16384]{2,1,0:T(2,128)(2,1)}, u32[]{:S(2)}, u32[]{:S(2)}) async-start(bf16[8,2,16384]{2,1,0:T(2,128)(2,1)} %reshape.412), calls=%async_computation.3 | async-start | bytes 1048576 | tf_op jit(solution)/shard_map/all_to_all | solution.py:201
  125.2 7.7 %copy-start.35 = (f32[4]{0:T(128)S(1)}, f32[4]{0:T(128)}, u32[]{:S(2)}) copy-start(f32[4]{0:T(128)} %param.29) | copy-start | bytes 52
  125.2 7.7 %copy-start.32 = (f32[5,256]{1,0:T(8,128)S(1)}, f32[5,256]{1,0:T(8,128)}, u32[]{:S(2)}) copy-start(f32[5,256]{1,0:T(8,128)} %param.27) | copy-start | bytes 15364
  125.2 7.7 %copy-start.30 = (f32[5,256]{1,0:T(8,128)S(1)}, f32[5,256]{1,0:T(8,128)}, u32[]{:S(2)}) copy-start(f32[5,256]{1,0:T(8,128)} %param.25) | copy-start | bytes 15364
  125.3 8.1 %copy-start.29 = (f32[1,1024,4]{1,2,0:T(4,128)S(1)}, f32[1,1024,4]{1,2,0:T(4,128)}, u32[]{:S(2)}) copy-start(f32[1,1024,4]{1,2,0:T(4,128)} %param.24) | copy-start | bytes 49156
  125.3 8.1 %copy-start.33 = (f32[4]{0:T(128)S(1)}, f32[4]{0:T(128)}, u32[]{:S(2)}) copy-start(f32[4]{0:T(128)} %param.28) | copy-start | bytes 52
  126.4 51.2 %all-to-all-start.4 = ((bf16[8,2,32768]{2,1,0:T(2,128)(2,1)}), bf16[8,2,32768]{2,1,0:T(2,128)(2,1)S(1)}, u32[]{:S(2)}, u32[]{:S(2)}) async-start(bf16[8,2,32768]{2,1,0:T(2,128)(2,1)} %reshape.406), calls=%async_computation.4 | async-start | bytes 2097152 | tf_op jit(solution)/shard_map/all_to_all | solution.py:198
  175.4 9.0 %copy-start.24 = (bf16[4,2,32768]{2,1,0:T(2,128)(2,1)S(1)}, bf16[4,2,32768]{2,1,0:T(2,128)(2,1)}, u32[]{:S(2)}) copy-start(bf16[4,2,32768]{2,1,0:T(2,128)(2,1)} %copy-done.23) | copy-start | bytes 1572868
  177.7 31.2 %all-to-all-start.2 = ((bf16[8,2,32768]{2,1,0:T(2,128)(2,1)}), bf16[8,2,32768]{2,1,0:T(2,128)(2,1)}, u32[]{:S(2)}, u32[]{:S(2)}) async-start(bf16[8,2,32768]{2,1,0:T(2,128)(2,1)} %reshape.404), calls=%async_computation.2 | async-start | bytes 2097152 | tf_op jit(solution)/shard_map/all_to_all | solution.py:199
  313.5 41.7 %all-to-all-start.6 = ((bf16[8,2,32768]{2,1,0:T(2,128)(2,1)}), bf16[8,2,32768]{2,1,0:T(2,128)(2,1)}, u32[]{:S(2)}, u32[]{:S(2)}) async-start(bf16[8,2,32768]{2,1,0:T(2,128)(2,1)} %reshape.414), calls=%async_computation.6 | async-start | bytes 2097152 | tf_op jit(solution)/shard_map/all_to_all | solution.py:258
  355.2 33.5 %all-to-all-start.5 = ((bf16[8,2,32768]{2,1,0:T(2,128)(2,1)}), bf16[8,2,32768]{2,1,0:T(2,128)(2,1)}, u32[]{:S(2)}, u32[]{:S(2)}) async-start(bf16[8,2,32768]{2,1,0:T(2,128)(2,1)} %reshape.416), calls=%async_computation.5 | async-start | bytes 2097152 | tf_op jit(solution)/shard_map/all_to_all | solution.py:251
  388.8 19.5 %all-to-all-start.8 = ((bf16[8,2,256]{2,1,0:T(2,128)(2,1)}), bf16[8,2,256]{2,1,0:T(2,128)(2,1)S(1)}, u32[]{:S(2)}, u32[]{:S(2)}) async-start(bf16[8,2,256]{2,1,0:T(2,128)(2,1)} %reshape.420), calls=%async_computation.8 | async-start | bytes 16384 | tf_op jit(solution)/shard_map/all_to_all | solution.py:265
  400.6 13.7 %copy-start.26 = (bf16[4,1,128,512]{3,2,0,1:T(8,128)(2,1)S(1)}, bf16[4,1,128,512]{3,2,0,1:T(8,128)(2,1)}, u32[]{:S(2)}) copy-start(bf16[4,1,128,512]{3,2,0,1:T(8,128)(2,1)} %copy.390) | copy-start | bytes 1572868
  408.3 26.1 %all-to-all-start.7 = ((bf16[8,2,16384]{2,1,0:T(2,128)(2,1)}), bf16[8,2,16384]{2,1,0:T(2,128)(2,1)S(1)}, u32[]{:S(2)}, u32[]{:S(2)}) async-start(bf16[8,2,16384]{2,1,0:T(2,128)(2,1)} %reshape.418), calls=%async_computation.7 | async-start | bytes 1048576 | tf_op jit(solution)/shard_map/all_to_all | solution.py:242
  414.3 84.2 %all-reduce.26.cloned.1.call-start = ((), (), s32[]{:S(2)}) async-start(), calls=%async_computation.11 | async-start | bytes 2097152 | tf_op jit(solution)/shard_map/psum | solution.py:289
  (24 other events, 103.8 us)
Sparse Core Ops, SparseCore 0:
  10.1 25.2 all-gather.1
  418.6 79.7 all-reduce.25
where the time goes:
time: 519 us; the launch traced here: 509 us
  other arithmetic  148 us (29%)
  local copies, waits for them, and re-layouts  125 us (24%)
  waiting for transfers between devices  78.6 us (15%)
  matrix products  76 us (15%)
  starting transfers between devices  58.5 us (11%)
  between operations  15.7 us (3%)
  blocking collectives  7.34 us (1%)
    unnamed x15, other arithmetic  108 us
    psum x1, waiting for transfers between devices, local(): total_grad = lax.psum(local_rows, 'sp')  58.7 us
    unnamed x111, local copies, waits for them, and re-layouts  46.7 us
    reshape x2, local copies, waits for them, and re-layouts, spread_heads(): return copied.reshape(1, tokens, HEADS * STATE)  33.5 us
    dot_general x3, matrix products, one_channel_scan(): jnp.einsum('ktn,ksn->kts', reading, keyed, precision=highest) * within  17.2 us
    all_to_all x1, waiting for transfers between devices, local(): lax.all_to_all(jnp.transpose(source_derivative, (1, 0, 2)).reshape(1, win...  17 us
    another operation x8, other arithmetic  14.2 us
    dot_general x3, matrix products, one_channel_scan(): jnp.einsum('ksn,ksp->knp', keyed * weight_fwd[:, :, None], driven, precis...  12.4 us
  transfers between devices with their start and end apart: 12, of which 3 were waited for; matrix products, arithmetic and copies ran while one was open for 47% of the time, Pallas kernels for 0%

commit v1 on v0

--- a/solution.py
+++ b/solution.py
@@ -286,7 +286,7 @@
     all_columns = column_block.reshape(data_devices * tokens, width_in // data_devices)
     all_grads = lax.all_gather(gradients, "dp", axis=0, tiled=True)
     local_rows = jnp.einsum("td,tc->dc", all_columns, all_grads, preferred_element_type=jnp.float32)
-    total_grad = lax.psum(local_rows, "sp")
+    total_grad = jnp.sum(lax.all_gather(local_rows, "sp"), axis=0)
     return (
         d_hidden.reshape(1, tokens, width_in),
         back_x,

time: 519 us -> 558 us (1.075)
  local copies, waits for them, and re-layouts: 125 us -> 153 us
  other arithmetic: 148 us -> 155 us
    psum x1 -> x0, waiting for transfers between devices: 58.7 us -> none  [local(): total_grad = lax.psum(local_rows, 'sp')]
    all_gather x0 -> x1, waiting for transfers between devices: none -> 39.4 us  [local(): total_grad = jnp.sum(lax.all_gather(local_rows, 'sp'), axis=0)]
    unnamed x111 -> x108, local copies, waits for them, and re-layouts: 46.7 us -> 72.5 us
    all_to_all x1, waiting for transfers between devices: 17 us -> 29.2 us  [local(): lax.all_to_all(jnp.transpose(source_derivative, (1, 0, 2)).reshape(1, win...]
    all_to_all x1, waiting for transfers between devices: 0.01 us -> 9.42 us  [local(): lax.all_to_all(jnp.transpose(writer_derivative, (1, 0, 2)).reshape(1, win...]
  transfers between devices with their start and end apart: 12 -> 12, of which waited for: 3 -> 4; matrix products, arithmetic and copies ran while one was open for 47% -> 64% of each run, Pallas kernels for 0% -> 0%
where the time goes in v1:
time: 558 us; the launch traced here: 550 us
  other arithmetic  155 us (28%)
  local copies, waits for them, and re-layouts  153 us (27%)
  waiting for transfers between devices  81.5 us (15%)
  matrix products  79.7 us (14%)
  starting transfers between devices  58 us (10%)
  between operations  15.4 us (3%)
  blocking collectives  7.8 us (1%)
    unnamed x15, other arithmetic  109 us
    unnamed x108, local copies, waits for them, and re-layouts  72.5 us
    all_gather x1, waiting for transfers between devices, local(): total_grad = jnp.sum(lax.all_gather(local_rows, 'sp'), axis=0)  39.4 us
    reshape x2, local copies, waits for them, and re-layouts, spread_heads(): return copied.reshape(1, tokens, HEADS * STATE)  33.5 us
    all_to_all x1, waiting for transfers between devices, local(): lax.all_to_all(jnp.transpose(source_derivative, (1, 0, 2)).reshape(1, win...  29.2 us
    dot_general x3, matrix products, one_channel_scan(): jnp.einsum('ktn,ksn->kts', reading, keyed, precision=highest) * within  21.2 us
    another operation x8, other arithmetic  14.3 us
    dot_general x3, matrix products, one_channel_scan(): jnp.einsum('ksn,ksp->knp', keyed * weight_bwd[:, :, None], driven, precis...  11.2 us
  transfers between devices with their start and end apart: 12, of which 4 were waited for; matrix products, arithmetic and copies ran while one was open for 64% of the time, Pallas kernels for 0%

profile of v1, /device:TPU:0, one launch (start us, length us, event | category | flops | bytes accessed | tf_op | source)
XLA Modules:
  0.0 550.4 jit_solution(6040868372961339566)
XLA Ops:
  11.8 7.3 %all-to-all-start.1 = ((bf16[8,2,256]{2,1,0:T(2,128)(2,1)}), bf16[8,2,256]{2,1,0:T(2,128)(2,1)S(1)}, u32[]{:S(2)}, u32[]{:S(2)}) async-start(bf16[8,2,256]{2,1,0:T(2,128)(2,1)} %reshape.409), calls=%async_computation.1 | async-start | bytes 16384 | tf_op jit(solution)/shard_map/all_to_all | solution.py:200
  23.9 12.3 %reduce.14 = bf16[2048,128]{1,0:T(8,128)(2,1)} reduce(bf16[2048,1,128]{2,1,0:T(2,128)(2,1)S(1)} %bitcast.417, bf16[]{:T(256)} %broadcast.265), dimensions={1}, to_apply=%bitcast.309.reduce_sub_computation | reduce | bytes 1048578
  38.2 6.6 %all-to-all-start = ((bf16[8,2,16384]{2,1,0:T(2,128)(2,1)}), bf16[8,2,16384]{2,1,0:T(2,128)(2,1)}, u32[]{:S(2)}, u32[]{:S(2)}) async-start(bf16[8,2,16384]{2,1,0:T(2,128)(2,1)} %reshape.411), calls=%async_computation | async-start | bytes 1048576 | tf_op jit(solution)/shard_map/all_to_all | solution.py:197
  51.8 11.6 %reduce.13 = bf16[2048,128]{1,0:T(8,128)(2,1)S(1)} reduce(bf16[2048,1,128]{2,1,0:T(2,128)(2,1)S(1)} %bitcast.414, bf16[]{:T(256)} %broadcast.265), dimensions={1}, to_apply=%bitcast.311.reduce_sub_computation | reduce | bytes 1048578
  64.4 6.2 %all-to-all-start.3 = ((bf16[8,2,16384]{2,1,0:T(2,128)(2,1)}), bf16[8,2,16384]{2,1,0:T(2,128)(2,1)}, u32[]{:S(2)}, u32[]{:S(2)}) async-start(bf16[8,2,16384]{2,1,0:T(2,128)(2,1)} %reshape.413), calls=%async_computation.3 | async-start | bytes 1048576 | tf_op jit(solution)/shard_map/all_to_all | solution.py:201
  73.5 16.7 %copy.533 = bf16[1,128,4096]{1,0,2:T(2,128)(2,1)S(1)} copy(bf16[1,128,4096]{1,2,0:T(8,128)(2,1)S(1)} %bitcast.403) | data formatting | bytes 2097152 | tf_op jit(solution)/shard_map/reshape | solution.py:150
  90.2 22.4 %reduce.11 = bf16[4096,128]{1,0:T(8,128)(2,1)S(1)} reduce(bf16[4096,1,128]{2,1,0:T(2,128)(2,1)S(1)} %bitcast.397, bf16[]{:T(256)} %broadcast.265), dimensions={1}, to_apply=%bitcast.369.reduce_sub_computation | reduce | bytes 2097154
  113.8 6.4 %all-to-all-start.4 = ((bf16[8,2,32768]{2,1,0:T(2,128)(2,1)}), bf16[8,2,32768]{2,1,0:T(2,128)(2,1)S(1)}, u32[]{:S(2)}, u32[]{:S(2)}) async-start(bf16[8,2,32768]{2,1,0:T(2,128)(2,1)} %reshape.407), calls=%async_computation.4 | async-start | bytes 2097152 | tf_op jit(solution)/shard_map/all_to_all | solution.py:198
  121.1 11.5 %reduce.19 = bf16[2048,128]{1,0:T(8,128)(2,1)S(1)} reduce(bf16[2048,1,128]{2,1,0:T(2,128)(2,1)S(1)} %bitcast.412, bf16[]{:T(256)} %broadcast.265), dimensions={1}, to_apply=%bitcast.321.reduce_sub_computation | reduce | bytes 1048578
  135.8 16.7 %copy.534 = bf16[1,128,4096]{1,0,2:T(2,128)(2,1)S(1)} copy(bf16[1,128,4096]{1,2,0:T(8,128)(2,1)S(1)} %bitcast.404) | data formatting | bytes 2097152 | tf_op jit(solution)/shard_map/reshape | solution.py:150
  152.6 23.4 %reduce.10 = bf16[4096,128]{1,0:T(8,128)(2,1)} reduce(bf16[4096,1,128]{2,1,0:T(2,128)(2,1)S(1)} %bitcast.398, bf16[]{:T(256)} %broadcast.265), dimensions={1}, to_apply=%bitcast.370.reduce_sub_computation | reduce | bytes 2097154
  178.2 6.5 %all-to-all-start.2 = ((bf16[8,2,32768]{2,1,0:T(2,128)(2,1)}), bf16[8,2,32768]{2,1,0:T(2,128)(2,1)}, u32[]{:S(2)}, u32[]{:S(2)}) async-start(bf16[8,2,32768]{2,1,0:T(2,128)(2,1)} %reshape.405), calls=%async_computation.2 | async-start | bytes 2097152 | tf_op jit(solution)/shard_map/all_to_all | solution.py:199
  280.0 6.1 %copy.366 = bf16[1,1024,512]{2,0,1:T(2,128)(2,1)} copy(bf16[1,1024,512]{1,2,0:T(8,128)(2,1)} %bitcast.419) | data formatting | bytes 2097152 | tf_op jit(solution)/shard_map/reshape | solution.py:259
  286.1 9.0 %reduce.15 = bf16[1024,512]{1,0:T(8,128)(2,1)} reduce(bf16[1024,1,512]{2,1,0:T(2,128)(2,1)} %bitcast.399, bf16[]{:T(256)} %broadcast.265), dimensions={1}, to_apply=%bitcast.313.reduce_sub_computation | reduce | bytes 2097154
  302.2 8.4 %add_add_fusion.1 = f32[4,8,128,128]{3,2,1,0:T(8,128)} fusion(f32[4,8,128,128]{3,2,1,0:T(8,128)} %fusion.90, f32[4,8,128,128]{3,2,1,0:T(8,128)} %get-tuple-element.110, f32[4,8,128,128]{3,2,1,0:T(8,128)} %bitcast.385, f32[4,8,128,128]{3,2,1,0:T(8,128)} %fusion.88, f32[4,8,128]{2,1,0:T(8,128)S(1)} %broadcast_add_fusion, ...), kind=kOutput, calls=%fused_computation.65 | convolution fusion | flops 809500672 | bytes 10534912 | tf_op jit(solution)/shard_map/vmap(transpose(jvp(ktn,ksn->kts)))/dot_general | solution.py:54
  320.4 6.2 %copy.353 = bf16[1,1024,512]{2,0,1:T(2,128)(2,1)} copy(bf16[1,1024,512]{1,2,0:T(8,128)(2,1)} %bitcast.420) | data formatting | bytes 2097152 | tf_op jit(solution)/shard_map/reshape | solution.py:252
  326.6 9.1 %reduce.16 = bf16[1024,512]{1,0:T(8,128)(2,1)} reduce(bf16[1024,1,512]{2,1,0:T(2,128)(2,1)} %bitcast.400, bf16[]{:T(256)} %broadcast.265), dimensions={1}, to_apply=%bitcast.315.reduce_sub_computation | reduce | bytes 2097154
  361.1 9.4 %all-to-all-done.5 = bf16[8,2,32768]{2,1,0:T(2,128)(2,1)} async-done(((bf16[8,2,32768]{2,1,0:T(2,128)(2,1)}), bf16[8,2,32768]{2,1,0:T(2,128)(2,1)}, u32[]{:S(2)}, u32[]{:S(2)}) %all-to-all-start.5) | async-done | bytes 1048608 | tf_op jit(solution)/shard_map/all_to_all | solution.py:251
  384.3 7.8 %all_gather.13 = bf16[512,512]{0,1:T(8,128)(2,1)S(1)} all-gather(bf16[128,512]{0,1:T(8,128)(2,1)S(1)} %pad_maximum_fusion.1), channel_id=1, replica_groups=mesh['sp'=8,'dp'=4] {'dp'}, dimensions={0}, use_global_device_ids=true | all-gather | bytes 655360 | tf_op jit(solution)/shard_map/all_gather | solution.py:287
  402.8 8.5 %fusion.208 = (f32[4,8,128]{2,1,0:T(8,128)S(1)}, f32[4,8,128]{2,1,0:T(8,128)S(1)}, f32[4,8,128,128]{3,2,1,0:T(8,128)}) fusion(f32[4,8,128,128]{3,2,1,0:T(8,128)} %fusion.88, f32[4,8,128,128]{3,2,1,0:T(8,128)} %bitcast.386, f32[4,8,128,128]{3,2,1,0:T(8,128)S(1)} %bitcast.380, f32[4,8,128]{2,1,0:T(8,128)S(1)} %broadcast_add_fusion), kind=kOutput, calls=%fused_computation.323 | convolution fusion | flops 812113920 | bytes 8437760 | tf_op jit(solution)/shard_map/vmap(jvp(ktn,ksn->kts))/dot_general | solution.py:54
  444.4 6.0 %all-to-all-start.7 = ((bf16[8,2,16384]{2,1,0:T(2,128)(2,1)}), bf16[8,2,16384]{2,1,0:T(2,128)(2,1)S(1)}, u32[]{:S(2)}, u32[]{:S(2)}) async-start(bf16[8,2,16384]{2,1,0:T(2,128)(2,1)} %reshape.419), calls=%async_computation.7 | async-start | bytes 1048576 | tf_op jit(solution)/shard_map/all_to_all | solution.py:242
  452.0 29.2 %all-to-all-done.7 = bf16[8,2,16384]{2,1,0:T(2,128)(2,1)S(1)} async-done(((bf16[8,2,16384]{2,1,0:T(2,128)(2,1)}), bf16[8,2,16384]{2,1,0:T(2,128)(2,1)S(1)}, u32[]{:S(2)}, u32[]{:S(2)}) %all-to-all-start.7) | async-done | bytes 524320 | tf_op jit(solution)/shard_map/all_to_all | solution.py:242
  486.7 39.4 %all-gather.6.cloned.1.call-done = f32[4096,512]{0,1:T(8,128)} async-done(((f32[512,512]{0,1:T(8,128)}), f32[4096,512]{0,1:T(8,128)}) %all-gather.6.cloned.1.call-update) | async-done | bytes 8388624 | tf_op jit(solution)/shard_map/all_gather | solution.py:289
  526.0 11.5 %copy.416 = f32[64,8,8,512]{3,2,1,0:T(8,128)S(1)} copy(f32[64,8,8,512]{3,1,2,0:T(8,128)} %bitcast.396) | data formatting | bytes 16777216
  (248 shorter events, 236.8 us)
Async XLA Ops:
  7.2 13.8 %copy-start.22 = (bf16[1,128,2048]{2,1,0:T(8,128)(2,1)S(1)}, bf16[1,128,2048]{2,1,0:T(8,128)(2,1)}, u32[]{:S(2)}) copy-start(bf16[1,128,2048]{2,1,0:T(8,128)(2,1)} %param.21) | copy-start | bytes 1572868
  7.2 63.7 %all-gather.4.cloned.1.call-start = ((), (), s32[]{:S(2)}) async-start(), calls=%async_computation.10 | async-start | bytes 2621440 | tf_op jit(solution)/shard_map/all_gather | solution.py:181
  9.1 11.9 %copy-start.21 = (bf16[1,128,2048]{2,1,0:T(8,128)(2,1)S(1)}, bf16[1,128,2048]{2,1,0:T(8,128)(2,1)}, u32[]{:S(2)}) copy-start(bf16[1,128,2048]{2,1,0:T(8,128)(2,1)} %param.20) | copy-start | bytes 1572868
  11.8 26.4 %all-to-all-start.1 = ((bf16[8,2,256]{2,1,0:T(2,128)(2,1)}), bf16[8,2,256]{2,1,0:T(2,128)(2,1)S(1)}, u32[]{:S(2)}, u32[]{:S(2)}) async-start(bf16[8,2,256]{2,1,0:T(2,128)(2,1)} %reshape.409), calls=%async_computation.1 | async-start | bytes 16384 | tf_op jit(solution)/shard_map/all_to_all | solution.py:200
  36.2 9.0 %copy-start.29 = (f32[5,256]{1,0:T(8,128)S(1)}, f32[5,256]{1,0:T(8,128)}, u32[]{:S(2)}) copy-start(f32[5,256]{1,0:T(8,128)} %param.26) | copy-start | bytes 15364
  38.2 26.2 %all-to-all-start = ((bf16[8,2,16384]{2,1,0:T(2,128)(2,1)}), bf16[8,2,16384]{2,1,0:T(2,128)(2,1)}, u32[]{:S(2)}, u32[]{:S(2)}) async-start(bf16[8,2,16384]{2,1,0:T(2,128)(2,1)} %reshape.411), calls=%async_computation | async-start | bytes 1048576 | tf_op jit(solution)/shard_map/all_to_all | solution.py:197
  51.8 19.0 %copy-start.23 = (bf16[1,128,2048]{2,1,0:T(8,128)(2,1)S(1)}, bf16[1,128,2048]{2,1,0:T(8,128)(2,1)}, u32[]{:S(2)}) copy-start(bf16[1,128,2048]{2,1,0:T(8,128)(2,1)} %param.16) | copy-start | bytes 1572868
  64.4 49.4 %all-to-all-start.3 = ((bf16[8,2,16384]{2,1,0:T(2,128)(2,1)}), bf16[8,2,16384]{2,1,0:T(2,128)(2,1)}, u32[]{:S(2)}, u32[]{:S(2)}) async-start(bf16[8,2,16384]{2,1,0:T(2,128)(2,1)} %reshape.413), calls=%async_computation.3 | async-start | bytes 1048576 | tf_op jit(solution)/shard_map/all_to_all | solution.py:201
  112.6 7.6 %copy-start.24 = (bf16[1,128,2048]{2,1,0:T(8,128)(2,1)S(1)}, bf16[1,128,2048]{2,1,0:T(8,128)(2,1)}, u32[]{:S(2)}) copy-start(bf16[1,128,2048]{2,1,0:T(8,128)(2,1)} %param.16) | copy-start | bytes 1572868
  113.8 7.2 %copy-start.33 = (f32[4]{0:T(128)S(1)}, f32[4]{0:T(128)}, u32[]{:S(2)}) copy-start(f32[4]{0:T(128)} %param.29) | copy-start | bytes 52
  113.8 7.2 %copy-start.30 = (f32[5,256]{1,0:T(8,128)S(1)}, f32[5,256]{1,0:T(8,128)}, u32[]{:S(2)}) copy-start(f32[5,256]{1,0:T(8,128)} %param.27) | copy-start | bytes 15364
  113.8 7.3 %copy-start.28 = (f32[5,256]{1,0:T(8,128)S(1)}, f32[5,256]{1,0:T(8,128)}, u32[]{:S(2)}) copy-start(f32[5,256]{1,0:T(8,128)} %param.25) | copy-start | bytes 15364
  113.8 64.4 %all-to-all-start.4 = ((bf16[8,2,32768]{2,1,0:T(2,128)(2,1)}), bf16[8,2,32768]{2,1,0:T(2,128)(2,1)S(1)}, u32[]{:S(2)}, u32[]{:S(2)}) async-start(bf16[8,2,32768]{2,1,0:T(2,128)(2,1)} %reshape.407), calls=%async_computation.4 | async-start | bytes 2097152 | tf_op jit(solution)/shard_map/all_to_all | solution.py:198
  120.2 13.6 %copy-start.27 = (f32[1,1024,4]{1,2,0:T(4,128)S(1)}, f32[1,1024,4]{1,2,0:T(4,128)}, u32[]{:S(2)}) copy-start(f32[1,1024,4]{1,2,0:T(4,128)} %param.24) | copy-start | bytes 49156
  120.2 13.6 %copy-start.31 = (f32[4]{0:T(128)S(1)}, f32[4]{0:T(128)}, u32[]{:S(2)}) copy-start(f32[4]{0:T(128)} %param.28) | copy-start | bytes 52
  178.2 10.3 %copy-start.18 = (bf16[8,2,32768]{2,1,0:T(2,128)(2,1)}, bf16[8,2,32768]{2,1,0:T(2,128)(2,1)S(1)}, u32[]{:S(2)}) copy-start(bf16[8,2,32768]{2,1,0:T(2,128)(2,1)S(1)} %all-to-all-done.4) | copy-start | bytes 3145732
  178.2 30.3 %all-to-all-start.2 = ((bf16[8,2,32768]{2,1,0:T(2,128)(2,1)}), bf16[8,2,32768]{2,1,0:T(2,128)(2,1)}, u32[]{:S(2)}, u32[]{:S(2)}) async-start(bf16[8,2,32768]{2,1,0:T(2,128)(2,1)} %reshape.405), calls=%async_computation.2 | async-start | bytes 2097152 | tf_op jit(solution)/shard_map/all_to_all | solution.py:199
  208.4 89.3 %all-to-all-start.9 = ((bf16[4,2,32768]{2,1,0:T(2,128)(2,1)}), bf16[4,2,32768]{2,1,0:T(2,128)(2,1)}, u32[]{:S(2)}, u32[]{:S(2)}) async-start(bf16[4,2,32768]{2,1,0:T(2,128)(2,1)} %reshape.423), calls=%async_computation.9 | async-start | bytes 1048576 | tf_op jit(solution)/shard_map/all_to_all | solution.py:285
  297.7 40.6 %all-to-all-start.6 = ((bf16[8,2,32768]{2,1,0:T(2,128)(2,1)}), bf16[8,2,32768]{2,1,0:T(2,128)(2,1)}, u32[]{:S(2)}, u32[]{:S(2)}) async-start(bf16[8,2,32768]{2,1,0:T(2,128)(2,1)} %reshape.415), calls=%async_computation.6 | async-start | bytes 2097152 | tf_op jit(solution)/shard_map/all_to_all | solution.py:258
  338.3 32.2 %all-to-all-start.5 = ((bf16[8,2,32768]{2,1,0:T(2,128)(2,1)}), bf16[8,2,32768]{2,1,0:T(2,128)(2,1)}, u32[]{:S(2)}, u32[]{:S(2)}) async-start(bf16[8,2,32768]{2,1,0:T(2,128)(2,1)} %reshape.417), calls=%async_computation.5 | async-start | bytes 2097152 | tf_op jit(solution)/shard_map/all_to_all | solution.py:251
  344.3 181.7 %all-gather.6.cloned.1.call-start = ((), (), s32[]{:S(2)}) async-start(), calls=%async_computation.11 | async-start | bytes 9437184 | tf_op jit(solution)/shard_map/all_gather | solution.py:289
  381.4 10.6 %copy-start.25 = (bf16[4,1,128,512]{3,2,0,1:T(8,128)(2,1)S(1)}, bf16[4,1,128,512]{3,2,0,1:T(8,128)(2,1)}, u32[]{:S(2)}) copy-start(bf16[4,1,128,512]{3,2,0,1:T(8,128)(2,1)} %copy.384) | copy-start | bytes 1572868
  433.0 11.4 %all-to-all-start.8 = ((bf16[8,2,256]{2,1,0:T(2,128)(2,1)}), bf16[8,2,256]{2,1,0:T(2,128)(2,1)S(1)}, u32[]{:S(2)}, u32[]{:S(2)}) async-start(bf16[8,2,256]{2,1,0:T(2,128)(2,1)} %reshape.421), calls=%async_computation.8 | async-start | bytes 16384 | tf_op jit(solution)/shard_map/all_to_all | solution.py:265
  444.4 36.9 %all-to-all-start.7 = ((bf16[8,2,16384]{2,1,0:T(2,128)(2,1)}), bf16[8,2,16384]{2,1,0:T(2,128)(2,1)S(1)}, u32[]{:S(2)}, u32[]{:S(2)}) async-start(bf16[8,2,16384]{2,1,0:T(2,128)(2,1)} %reshape.419), calls=%async_computation.7 | async-start | bytes 1048576 | tf_op jit(solution)/shard_map/all_to_all | solution.py:242
  (22 other events, 76.5 us)
Sparse Core Ops, SparseCore 0:
  10.1 25.2 all-gather.3
  393.6 132.3 all-gather.5
